TPU v7x, 512 devices: a whole 4x4x16 slice. The times are simulated.
512 devices in a mesh: sp: 32 (over z, core), tp: 16 (over y, x).
Axes of the slice: x: 4, y: 4, z: 16, core: 2. Of those that a mesh axis runs over, the one named last changes fastest.
Arguments:
- residual: bfloat16 [3584, 2048], P('sp'), may hold values from -1.5 to 1.5
- latent: bfloat16 [3584, 512], P('sp'), may hold values from -6 to 6
- rot_key: bfloat16 [3584, 64], P('sp'), may hold values from -6 to 6
- latent_norm_scale: float32 [512], replicated, may hold values from 0.1 to 1.9
- query_wide: bfloat16 [3584, 3072], P('sp', 'tp'), may hold values from -210 to 210
- query_narrow: bfloat16 [3584, 2048], P('sp', 'tp'), may hold values from -210 to 210
- large_key_lift: bfloat16 [512, 2048], P(None, 'tp'), may hold values from -0.25 to 0.25
- large_value_lift: bfloat16 [512, 2048], P(None, 'tp'), may hold values from -0.25 to 0.25
- small_key_lift: bfloat16 [512, 1024], P(None, 'tp'), may hold values from -0.25 to 0.25
- small_value_lift: bfloat16 [512, 1024], P(None, 'tp'), may hold values from -0.25 to 0.25
- out_wide: bfloat16 [2048, 2048], P('tp'), may hold values from -0.5 to 0.5
- out_narrow: bfloat16 [1024, 2048], P('tp'), may hold values from -0.75 to 0.75
- mix_gain: float32 [2048], replicated, may hold values from 0.1 to 1.9
- router_group: bfloat16 [2048, 4], replicated, may hold values from -0.125 to 0.125
- router_expert: bfloat16 [2048, 32], replicated, may hold values from -0.125 to 0.125
- expert_ids: int32 [3584, 2], P('sp'), may hold values from 0 to 31, all different within a row; in each aligned block of 112 rows (0 to 111, 112 to 223, ...) at most 16 rows name the same one
- expert_gate_w: bfloat16 [32, 2048, 4096], P('sp', None, 'tp'), may hold values from -0.125 to 0.125
- expert_up_w: bfloat16 [32, 2048, 4096], P('sp', None, 'tp'), may hold values from -0.125 to 0.125
- expert_down_w: bfloat16 [32, 4096, 2048], P('sp', 'tp'), may hold values from -0.375 to 0.375
Outputs:
- updated: bfloat16 [3584, 2048], P('sp', 'tp')
Inputs may be any that keep to these rules, and one draw needn't show every extreme that they name: `expert_ids`: each row names two different experts; the rows of one index of sp name no expert more than 16 times, a bound that some expert reaches in some of these blocks.
All inputs are finite; a program needn't handle non-finite values.
Results may differ from a plain program's by a relative error of at most 0.024.
The roundings to bfloat16 on the way count: a program that leaves them out, or rounds other values in their place, can miss the bound.
Values may be sent and summed in bfloat16 or wider, within the bound.
A program may use at most 64 MiB of HBM per device.

v0:
```python
import jax
import jax.numpy as jnp
from jax import lax
from jax.sharding import PartitionSpec as P

PLAIN_KEY_WIDTH = 128
LARGE_VALUE_SIZE = 128
SMALL_HEAD_WIDTH = 64
ROPE = 64


rope_base = 10000.0
epsilon = 1e-06
very_low = -1e30


def sent_together(arrays, axis, dim, along):
    columns = [a.reshape(*a.shape[:along], -1) for a in arrays]
    both = jnp.concatenate(columns, axis=along)
    out, at, done = (lax.all_gather(both, axis, axis=dim, tiled=True), 0, [])
    for a, column in zip(arrays, columns):
        section = out[..., at : at + column.shape[along]]
        done.append(section.reshape(*section.shape[:along], *a.shape[along:]))
        at += column.shape[along]
    return tuple(done)


def padded_to(lines, length):
    spare = -lines.shape[0] % length
    if not spare:
        return lines
    return jnp.concatenate([lines, jnp.zeros((spare, *lines.shape[1:]), lines.dtype)])


def joined_along(pieces, dim):
    shape = list(pieces.shape[1:])
    shape[dim] *= pieces.shape[0]
    return jnp.moveaxis(pieces, 0, dim).reshape(shape)


def sent_to_all(x, axis):
    copies = jnp.broadcast_to(x, (lax.axis_size(axis), *x.shape))
    return lax.all_to_all(copies, axis, split_axis=0, concat_axis=0, tiled=True)


def gathered_copies(x, axis, dim):
    return joined_along(sent_to_all(x, axis), dim)


def in_blocks(x, dim, length):
    before, after = (x.shape[:dim], x.shape[dim + 1 :])
    return jnp.moveaxis(x.reshape(*before, length, -1, *after), dim, 0)


def sum_at_owner(x, axis, dim):
    pieces = in_blocks(x, dim, lax.axis_size(axis))
    arrived = lax.all_to_all(pieces, axis, split_axis=0, concat_axis=0, tiled=True)
    return arrived.astype(jnp.float32).sum(axis=0)


def sum_by_parts(x, axes):
    lines = x.reshape(-1, x.shape[-1])
    padded = padded_to(lines, lax.axis_size(axes))
    whole = gathered_copies(sum_at_owner(padded, axes, 0).astype(jnp.bfloat16), axes, 0)
    return lax.slice_in_dim(whole, 0, len(lines)).reshape(x.shape).astype(jnp.float32)


def angle_table(positions, width):
    frequency = rope_base ** (-jnp.arange(0, width, 2, dtype=jnp.float32) / width)
    return positions.astype(jnp.float32)[:, None] * frequency[None, :]


def rotate(values, angles):
    half_width = values.shape[-1] // 2
    cosine = jnp.cos(angles)
    sine_part = jnp.sin(angles)
    front_half = values[..., :half_width]
    back_half = values[..., half_width:]
    return jnp.concatenate(
        [front_half * cosine - back_half * sine_part, front_half * sine_part + back_half * cosine],
        axis=-1,
    )


def rms_scale(values, gain):
    return values * lax.rsqrt(jnp.mean(values * values, axis=-1, keepdims=True) + epsilon) * gain


def roped_queries(query, plain_width, angles):
    row_count = query.shape[0]
    shaped = query.reshape(row_count, -1, plain_width + ROPE)
    turned = rotate(shaped[..., plain_width:].astype(jnp.float32), angles[:, None, :]).astype(
        jnp.bfloat16
    )
    return jnp.concatenate([shaped[..., :plain_width], turned], axis=-1)


def expand_keys(latent_rows, large_key_lift, large_value_lift, small_key_lift, small_value_lift):
    row_count = latent_rows.shape[0]

    def project(weight, head_width):
        product = jnp.dot(latent_rows, weight, preferred_element_type=jnp.float32).astype(
            jnp.bfloat16
        )
        return product.reshape(row_count, weight.shape[1] // head_width, head_width)

    return (
        project(large_key_lift, PLAIN_KEY_WIDTH),
        project(large_value_lift, LARGE_VALUE_SIZE),
        project(small_key_lift, SMALL_HEAD_WIDTH),
        project(small_value_lift, SMALL_HEAD_WIDTH),
    )


def attend_group(state, queries, plain_width, key_rows, values, key_rot, causal_mask):
    row_peak, weight_sum, summed = state
    score_scale = (plain_width + ROPE) ** (-0.5)
    scores = jnp.einsum(
        "qhd,khd->qhk", queries[..., :plain_width], key_rows, preferred_element_type=jnp.float32
    )
    scores = scores + jnp.einsum(
        "qhd,kd->qhk", queries[..., plain_width:], key_rot, preferred_element_type=jnp.float32
    )
    scores = scores * score_scale
    allowed = causal_mask[:, None, :]
    new_peak = jnp.maximum(row_peak, jnp.max(jnp.where(allowed, scores, very_low), axis=-1))
    weights = jnp.where(allowed, jnp.exp(scores - new_peak[..., None]), 0.0)
    weight_sum = jnp.sum(weights, axis=-1)
    summed = jnp.einsum(
        "qhk,khd->qhd", weights.astype(jnp.bfloat16), values, preferred_element_type=jnp.float32
    )
    return (new_peak, weight_sum, summed)


def shards(
    residual,
    latent,
    rot_key,
    latent_norm_scale,
    query_wide,
    query_narrow,
    large_key_lift,
    large_value_lift,
    small_key_lift,
    small_value_lift,
    out_wide,
    out_narrow,
    mix_gain,
    router_group,
    router_expert,
    expert_ids,
    expert_gate_w,
    expert_up_w,
    expert_down_w,
):
    tok_rows = latent.shape[0]
    positions = lax.axis_index("sp") * tok_rows + jnp.arange(tok_rows, dtype=jnp.int32)
    angles = angle_table(positions, ROPE)
    normed = rms_scale(latent.astype(jnp.float32), latent_norm_scale).astype(jnp.bfloat16)
    key_turned = rotate(rot_key.astype(jnp.float32), angles).astype(jnp.bfloat16)
    wide_queries = roped_queries(query_wide, PLAIN_KEY_WIDTH, angles)
    narrow_queries = roped_queries(query_narrow, SMALL_HEAD_WIDTH, angles)

    def empty_state(head_count, head_width):
        return (
            jnp.full((tok_rows, head_count), very_low, jnp.float32),
            jnp.zeros((tok_rows, head_count), jnp.float32),
            jnp.zeros((tok_rows, head_count, head_width), jnp.float32),
        )

    initial = (
        empty_state(wide_queries.shape[1], LARGE_VALUE_SIZE),
        empty_state(narrow_queries.shape[1], SMALL_HEAD_WIDTH),
    )
    own_keys = expand_keys(
        normed, large_key_lift, large_value_lift, small_key_lift, small_value_lift
    )
    pieces = sent_together(
        (own_keys[0], own_keys[1], own_keys[2], own_keys[3], key_turned), "sp", 0, 1
    )
    key_set = pieces[:4]
    key_rot = pieces[4]
    key_positions = jnp.arange(key_rot.shape[0], dtype=jnp.int32)
    causal_mask = positions[:, None] >= key_positions[None, :]
    wide_state = attend_group(
        initial[0], wide_queries, PLAIN_KEY_WIDTH, key_set[0], key_set[1], key_rot, causal_mask
    )
    narrow_state = attend_group(
        initial[1], narrow_queries, SMALL_HEAD_WIDTH, key_set[2], key_set[3], key_rot, causal_mask
    )

    def heads_out(state):
        return (state[2] / state[1][..., None]).astype(jnp.bfloat16).reshape(tok_rows, -1)

    partial_value = jnp.dot(heads_out(wide_state), out_wide, preferred_element_type=jnp.float32)
    partial_value = partial_value + jnp.dot(
        heads_out(narrow_state), out_narrow, preferred_element_type=jnp.float32
    )
    rounded_partial = lax.optimization_barrier(partial_value.astype(jnp.bfloat16)).astype(
        jnp.float32
    )
    attended = sum_by_parts(rounded_partial.astype(jnp.bfloat16), "tp")
    mixed = residual.astype(jnp.float32) + attended
    normal_rows = rms_scale(mixed, mix_gain).astype(jnp.bfloat16)
    group_count = router_group.shape[1]
    expert_count = router_expert.shape[1]
    group_prob = jax.nn.softmax(
        jnp.dot(normal_rows, router_group, preferred_element_type=jnp.float32), axis=-1
    )
    logits = jnp.dot(normal_rows, router_expert, preferred_element_type=jnp.float32)
    chosen_group = expert_ids[:, 0] // (expert_count // group_count)
    group_pick = jnp.sum(
        jnp.where(chosen_group[:, None] == jnp.arange(group_count)[None, :], group_prob, 0.0),
        axis=1,
    )
    expert_match = expert_ids[:, :, None] == jnp.arange(expert_count)[None, None, :]
    chosen_logits = jnp.sum(jnp.where(expert_match, logits[:, None, :], 0.0), axis=2)
    gates = group_pick[:, None] * jax.nn.softmax(chosen_logits, axis=-1)
    tp_size = lax.axis_size("tp")
    sp_size = lax.axis_size("sp")
    capacity = tp_size * max(1, 4 * tok_rows // (expert_count * tp_size))
    flat_ids = expert_ids.reshape(-1)
    one_hot = (flat_ids[:, None] == jnp.arange(expert_count)[None, :]).astype(jnp.int32)
    earlier = jnp.cumsum(one_hot, axis=0) - one_hot
    slot_index = jnp.sum(earlier * one_hot, axis=1)
    target = flat_ids * capacity + slot_index
    source_row = jnp.arange(flat_ids.shape[0], dtype=jnp.int32) // 2
    row_of_slot = jnp.zeros((expert_count * capacity,), jnp.int32).at[target].set(source_row)
    slot_used = jnp.zeros((expert_count * capacity,), jnp.bool_).at[target].set(True)
    outgoing = jnp.where(slot_used[:, None], normal_rows[row_of_slot], jnp.zeros((), jnp.bfloat16))
    outgoing = outgoing.reshape(expert_count, capacity, -1)
    share_slots = capacity // tp_size
    own_slots = lax.dynamic_slice_in_dim(
        outgoing, lax.axis_index("tp") * share_slots, share_slots, 1
    )
    arrived = lax.all_to_all(own_slots, "sp", split_axis=0, concat_axis=1, tiled=True)
    expert_rows = gathered_copies(arrived, "tp", 1)
    gate_part = jnp.einsum(
        "erd,edf->erf", expert_rows, expert_gate_w, preferred_element_type=jnp.float32
    )
    up_part = jnp.einsum(
        "erd,edf->erf", expert_rows, expert_up_w, preferred_element_type=jnp.float32
    )
    hidden = (jax.nn.silu(gate_part) * up_part).astype(jnp.bfloat16)
    down_part = jnp.einsum(
        "erf,efd->erd", hidden, expert_down_w, preferred_element_type=jnp.float32
    )
    rounded_down = lax.optimization_barrier(down_part.astype(jnp.bfloat16)).astype(jnp.float32)
    expert_out = sum_at_owner(rounded_down.astype(jnp.bfloat16), "tp", 2).astype(jnp.bfloat16)
    column_count = expert_out.shape[2]
    shaped_out = expert_out.reshape(expert_out.shape[0], tp_size, sp_size, -1, column_count)
    returned = lax.all_to_all(shaped_out, "sp", split_axis=2, concat_axis=0, tiled=True)
    returned = returned.reshape(expert_count * capacity, column_count)
    picked = returned[target].astype(jnp.float32).reshape(tok_rows, 2, column_count)
    combined = jnp.sum(picked * gates[:, :, None], axis=1)
    own_columns = lax.dynamic_slice_in_dim(
        mixed, lax.axis_index("tp") * column_count, column_count, 1
    )
    return (own_columns + combined).astype(jnp.bfloat16)


def solution(mesh):
    placed = (
        P("sp", None),
        P("sp", None),
        P("sp", None),
        P(),
        P("sp", "tp"),
        P("sp", "tp"),
        P(None, "tp"),
        P(None, "tp"),
        P(None, "tp"),
        P(None, "tp"),
        P("tp", None),
        P("tp", None),
        P(),
        P(),
        P(),
        P("sp", None),
        P("sp", None, "tp"),
        P("sp", None, "tp"),
        P("sp", "tp", None),
    )
    return jax.shard_map(
        shards, mesh=mesh, in_specs=placed, out_specs=P("sp", "tp"), check_vma=False
    )
```

profile of v0, /device:TPU:1, one launch (start us, length us, event | category | flops | bytes accessed | tf_op | source)
XLA Modules:
  0.0 285.6 jit_solution(499772698731304938)
XLA Ops:
  16.6 76.9 %all-gather.2.cloned.1.call-done = bf16[3584,448]{1,0:T(8,128)(2,1)} async-done(((bf16[112,448]{1,0:T(8,128)(2,1)}), bf16[3584,448]{1,0:T(8,128)(2,1)}) %all-gather.2.cloned.1.call-update) | async-done | bytes 3211280 | tf_op jit(solution)/shard_map/all_gather | solution.py:20
  93.4 1.6 convolution_bitcast_fusion.2
  95.1 1.7 fusion.1
  100.1 2.9 %fusion.37 = f32[112,2048]{1,0:T(8,128)} fusion(bf16[128,2048]{1,0:T(8,128)(2,1)S(1)} %copy-done.4, bf16[3584,448]{1,0:T(8,128)(2,1)} %all-gather.2.cloned.1.call-done, f32[112,1,3584]{2,0,1:T(8,128)S(1)} %fusion.1, f32[112]{0:T(128)S(1)} %broadcast_maximum_fusion.1, s32[112]{0:T(128)S(1)} %iota_add_fusion, f32[112]{0:T(128)S(1)} %get-tuple-element.6), kind=kOutput, calls=%fused_computation.55 | convolution fusion | flops 163115008 | bytes 3966272 | tf_op jit(solution)/shard_map/dot_general | solution.py:195
  103.0 3.3 %fusion.5 = bf16[112,2048]{1,0:T(8,128)(2,1)S(1)} fusion(f32[112,2048]{1,0:T(8,128)} %fusion.37, bf16[64,2048]{1,0:T(8,128)(2,1)S(1)} %copy-done.6, bf16[3584,448]{1,0:T(8,128)(2,1)} %all-gather.2.cloned.1.call-done, f32[112,1,3584]{2,0,1:T(8,128)} %copy-done.1, f32[112]{0:T(128)S(1)} %broadcast_maximum_fusion, s32[112]{0:T(128)S(1)} %iota_add_fusion, ...), kind=kOutput, calls=%fused_computation.15 | convolution fusion | flops 82819072 | bytes 4162880 | tf_op jit(solution)/shard_map/dot_general | solution.py:196
  107.3 6.5 %all-to-all-start = ((bf16[16,7,2048]{2,1,0:T(8,128)(2,1)}), bf16[16,7,2048]{2,1,0:T(8,128)(2,1)S(1)}, u32[]{:S(2)}, u32[]{:S(2)}) async-start(bf16[16,7,2048]{2,1,0:T(8,128)(2,1)} %reshape.407), calls=%async_computation | async-start | bytes 1048576 | tf_op jit(solution)/shard_map/all_to_all | solution.py:57
  113.8 1.3 scatter_custom_fusion.1
  115.2 1.4 scatter_custom_fusion
  116.6 8.0 %all-to-all-done = bf16[16,7,2048]{2,1,0:T(8,128)(2,1)S(1)} async-done(((bf16[16,7,2048]{2,1,0:T(8,128)(2,1)}), bf16[16,7,2048]{2,1,0:T(8,128)(2,1)S(1)}, u32[]{:S(2)}, u32[]{:S(2)}) %all-to-all-start) | async-done | bytes 458784 | tf_op jit(solution)/shard_map/all_to_all | solution.py:57
  125.6 3.6 %all-to-all-start.1 = ((bf16[16,7,2048]{2,1,0:T(8,128)(2,1)}), bf16[16,7,2048]{2,1,0:T(8,128)(2,1)S(1)}, u32[]{:S(2)}, u32[]{:S(2)}) async-start(bf16[16,7,2048]{2,1,0:T(8,128)(2,1)} %broadcast_in_dim.47), calls=%async_computation.1 | async-start | bytes 1048576 | tf_op jit(solution)/shard_map/all_to_all | solution.py:43
  129.3 10.0 %all-to-all-done.1 = bf16[16,7,2048]{2,1,0:T(8,128)(2,1)S(1)} async-done(((bf16[16,7,2048]{2,1,0:T(8,128)(2,1)}), bf16[16,7,2048]{2,1,0:T(8,128)(2,1)S(1)}, u32[]{:S(2)}, u32[]{:S(2)}) %all-to-all-start.1) | async-done | bytes 458784 | tf_op jit(solution)/shard_map/all_to_all | solution.py:43
  139.8 3.3 %gather_fusion = bf16[512,2048]{1,0:T(8,128)(2,1)} fusion(bf16[112,2048]{1,0:T(8,128)(2,1)S(1)} %multiply_convert_fusion, s32[1024]{0:T(1024)S(1)} %pad_clamp_fusion.1), kind=kCustom, calls=%fused_computation | custom fusion | bytes 4196352 | tf_op jit(solution)/shard_map/gather | solution.py:230
  143.1 1.6 broadcast_select_fusion
  145.2 1.4 reduce.9
  146.7 25.7 %all_to_all.47 = bf16[32,2,1024]{2,1,0:T(2,128)(2,1)S(1)} all-to-all(bf16[32,2,1024]{2,1,0:T(2,128)(2,1)S(1)} %reshape.458), channel_id=1, replica_groups=mesh['sp'=32,'tp'=16] {'sp'}, dimensions={0} | all-to-all | bytes 262144 | tf_op jit(solution)/shard_map/all_to_all | solution.py:236
  172.9 30.0 %all_to_all.48 = bf16[16,1,32,2048]{3,2,1,0:T(8,128)(2,1)S(1)} all-to-all(bf16[16,1,32,2048]{3,2,1,0:T(8,128)(2,1)S(1)} %broadcast_in_dim.95), channel_id=1, replica_groups=mesh['sp'=32,'tp'=16] {'tp'}, dimensions={0} | all-to-all | bytes 4194304 | tf_op jit(solution)/shard_map/all_to_all | solution.py:43
  204.2 1.5 fusion.19
  205.7 5.6 %fusion.4 = bf16[1,512,2048]{2,1,0:T(8,128)(2,1)} fusion(bf16[1,256,2048]{2,1,0:T(8,128)(2,1)S(1)} %copy-done, bf16[512,2048]{1,0:T(8,128)(2,1)} %bitcast.144, bf16[1,2048,256]{2,1,0:T(8,128)(2,1)} %param.36, f32[512,256]{1,0:T(8,128)} %fusion.19), kind=kOutput, calls=%fused_computation.13 | convolution fusion | flops 1075576832 | bytes 6815744 | tf_op jit(solution)/shard_map/erf,efd->erd/dot_general | solution.py:245
  211.4 3.4 %bitcast_bitcast_fusion = bf16[16,1,512,128]{3,2,1,0:T(8,128)(2,1)} fusion(bf16[1,512,2048]{2,1,0:T(8,128)(2,1)} %fusion.4), kind=kLoop, calls=%fused_computation.16 | loop fusion | bytes 4194304 | tf_op jit(solution)/shard_map/transpose | solution.py:52
  214.8 4.6 %all-to-all-start.4 = ((bf16[16,1,512,128]{3,2,1,0:T(8,128)(2,1)}), bf16[16,1,512,128]{3,2,1,0:T(8,128)(2,1)}, u32[]{:S(2)}, u32[]{:S(2)}) async-start(bf16[16,1,512,128]{3,2,1,0:T(8,128)(2,1)} %bitcast_bitcast_fusion), calls=%async_computation.4 | async-start | bytes 4194304 | tf_op jit(solution)/shard_map/all_to_all | solution.py:57
  220.0 25.6 %all-to-all-done.4 = bf16[16,1,512,128]{3,2,1,0:T(8,128)(2,1)} async-done(((bf16[16,1,512,128]{3,2,1,0:T(8,128)(2,1)}), bf16[16,1,512,128]{3,2,1,0:T(8,128)(2,1)}, u32[]{:S(2)}, u32[]{:S(2)}) %all-to-all-start.4) | async-done | bytes 2097184 | tf_op jit(solution)/shard_map/all_to_all | solution.py:57
  245.6 1.9 reduce_sum.123
  248.2 13.1 %all-to-all-start.5 = ((bf16[1,16,32,1,128]{4,1,3,0,2:T(8,128)(2,1)}), bf16[1,16,32,1,128]{4,1,3,0,2:T(8,128)(2,1)S(1)}, u32[]{:S(2)}, u32[]{:S(2)}) async-start(bf16[1,16,32,1,128]{4,1,3,0,2:T(8,128)(2,1)} %copy.72), calls=%async_computation.5 | async-start | bytes 262144 | tf_op jit(solution)/shard_map/all_to_all | solution.py:252
  261.5 15.6 %all-to-all-done.5 = bf16[1,16,32,1,128]{4,1,3,0,2:T(8,128)(2,1)S(1)} async-done(((bf16[1,16,32,1,128]{4,1,3,0,2:T(8,128)(2,1)}), bf16[1,16,32,1,128]{4,1,3,0,2:T(8,128)(2,1)S(1)}, u32[]{:S(2)}, u32[]{:S(2)}) %all-to-all-start.5) | async-done | bytes 131104 | tf_op jit(solution)/shard_map/all_to_all | solution.py:252
  (101 shorter events, 21.2 us)
Async XLA Ops:
  6.5 199.2 %copy-start = (bf16[1,256,2048]{2,1,0:T(8,128)(2,1)S(1)}, bf16[1,256,2048]{2,1,0:T(8,128)(2,1)}, u32[]{:S(2)}) copy-start(bf16[1,256,2048]{2,1,0:T(8,128)(2,1)} %param.37) | copy-start | bytes 3145732
  6.5 8.1 %copy-start.9 = (bf16[112,192]{0,1:T(8,128)(2,1)S(1)}, bf16[112,192]{0,1:T(8,128)(2,1)}, u32[]{:S(2)}) copy-start(bf16[112,192]{0,1:T(8,128)(2,1)} %param.23) | copy-start | bytes 129028
  6.5 8.2 %copy-start.11 = (s32[112,2]{0,1:T(2,128)S(1)}, s32[112,2]{0,1:T(2,128)}, u32[]{:S(2)}) copy-start(s32[112,2]{0,1:T(2,128)} %param.34) | copy-start | bytes 2692
  6.5 9.6 %copy-start.8 = (bf16[112,128]{1,0:T(8,128)(2,1)S(1)}, bf16[112,128]{1,0:T(8,128)(2,1)}, u32[]{:S(2)}) copy-start(bf16[112,128]{1,0:T(8,128)(2,1)} %param.24) | copy-start | bytes 86020
  6.5 86.9 %all-gather.2.cloned.1.call-start = ((), (), s32[]{:S(2)}) async-start(), calls=%async_computation.6 | async-start | bytes 3784704 | tf_op jit(solution)/shard_map/all_gather | solution.py:20
  95.1 2.3 copy-start.2
  98.7 1.2 copy-start.1
  98.7 1.4 copy-start.4
  100.1 2.9 %copy-start.6 = (bf16[64,2048]{1,0:T(8,128)(2,1)S(1)}, bf16[64,2048]{1,0:T(8,128)(2,1)}, u32[]{:S(2)}) copy-start(bf16[64,2048]{1,0:T(8,128)(2,1)} %param.30) | copy-start | bytes 786436
  107.3 17.4 %all-to-all-start = ((bf16[16,7,2048]{2,1,0:T(8,128)(2,1)}), bf16[16,7,2048]{2,1,0:T(8,128)(2,1)S(1)}, u32[]{:S(2)}, u32[]{:S(2)}) async-start(bf16[16,7,2048]{2,1,0:T(8,128)(2,1)} %reshape.407), calls=%async_computation | async-start | bytes 1048576 | tf_op jit(solution)/shard_map/all_to_all | solution.py:57
  124.7 14.6 %copy-start.5 = (bf16[112,2048]{1,0:T(8,128)(2,1)S(1)}, bf16[112,2048]{1,0:T(8,128)(2,1)}, u32[]{:S(2)}) copy-start(bf16[112,2048]{1,0:T(8,128)(2,1)} %param.19) | copy-start | bytes 1376260
  125.6 13.7 %all-to-all-start.1 = ((bf16[16,7,2048]{2,1,0:T(8,128)(2,1)}), bf16[16,7,2048]{2,1,0:T(8,128)(2,1)S(1)}, u32[]{:S(2)}, u32[]{:S(2)}) async-start(bf16[16,7,2048]{2,1,0:T(8,128)(2,1)} %broadcast_in_dim.47), calls=%async_computation.1 | async-start | bytes 1048576 | tf_op jit(solution)/shard_map/all_to_all | solution.py:43
  129.3 10.3 %copy-start.12 = (f32[2048]{0:T(1024)S(1)}, f32[2048]{0:T(1024)}, u32[]{:S(2)}) copy-start(f32[2048]{0:T(1024)} %param.31) | copy-start | bytes 24580
  172.9 31.3 %copy-start.13 = (bf16[1,2048,256]{2,1,0:T(8,128)(2,1)S(1)}, bf16[1,2048,256]{2,1,0:T(8,128)(2,1)}, u32[]{:S(2)}) copy-start(bf16[1,2048,256]{2,1,0:T(8,128)(2,1)} %param.35) | copy-start | bytes 3145732
  202.9 1.3 copy-start.3
  214.8 4.6 %copy-start.7 = (bf16[2048,32]{0,1:T(8,128)(2,1)S(1)}, bf16[2048,32]{0,1:T(8,128)(2,1)}, u32[]{:S(2)}) copy-start(bf16[2048,32]{0,1:T(8,128)(2,1)} %param.33) | copy-start | bytes 393220
  214.8 4.9 %copy-start.10 = (bf16[2048,4]{0,1:T(4,128)(2,1)S(1)}, bf16[2048,4]{0,1:T(4,128)(2,1)}, u32[]{:S(2)}) copy-start(bf16[2048,4]{0,1:T(4,128)(2,1)} %param.32) | copy-start | bytes 49156
  214.8 30.8 %all-to-all-start.4 = ((bf16[16,1,512,128]{3,2,1,0:T(8,128)(2,1)}), bf16[16,1,512,128]{3,2,1,0:T(8,128)(2,1)}, u32[]{:S(2)}, u32[]{:S(2)}) async-start(bf16[16,1,512,128]{3,2,1,0:T(8,128)(2,1)} %bitcast_bitcast_fusion), calls=%async_computation.4 | async-start | bytes 4194304 | tf_op jit(solution)/shard_map/all_to_all | solution.py:57
  248.2 29.0 %all-to-all-start.5 = ((bf16[1,16,32,1,128]{4,1,3,0,2:T(8,128)(2,1)}), bf16[1,16,32,1,128]{4,1,3,0,2:T(8,128)(2,1)S(1)}, u32[]{:S(2)}, u32[]{:S(2)}) async-start(bf16[1,16,32,1,128]{4,1,3,0,2:T(8,128)(2,1)} %copy.72), calls=%async_computation.5 | async-start | bytes 262144 | tf_op jit(solution)/shard_map/all_to_all | solution.py:252
Sparse Core Ops, SparseCore 0:
  14.7 78.6 all-gather.1
where the time goes:
time: 287 us; the launch traced here: 286 us
  waiting for transfers between devices  136 us (47%)
  blocking collectives  55.8 us (19%)
  starting transfers between devices  27.8 us (10%)
  matrix products  23.1 us (8%)
  local copies, waits for them, and re-layouts  18.7 us (7%)
  between operations  13.8 us (5%)
  other arithmetic  10.3 us (4%)
    all_gather x1, waiting for transfers between devices, sent_together(): out, at, done = (lax.all_gather(both, axis, axis=dim, tiled=True), 0, [])  76.9 us
    all_to_all x2, waiting for transfers between devices, sum_at_owner(): lax.all_to_all(pieces, axis, split_axis=0, concat_axis=0, tiled=True)  33.6 us
    all_to_all x1, blocking collectives, sent_to_all(): return lax.all_to_all(copies, axis, split_axis=0, concat_axis=0, tiled=True)  30 us
    all_to_all x1, blocking collectives, shards(): lax.all_to_all(own_slots, 'sp', split_axis=0, concat_axis=1, tiled=True)  25.7 us
    all_to_all x1, waiting for transfers between devices, shards(): lax.all_to_all(shaped_out, 'sp', split_axis=2, concat_axis=0, tiled=True)  15.6 us
    all_to_all x1, starting transfers between devices, shards(): lax.all_to_all(shaped_out, 'sp', split_axis=2, concat_axis=0, tiled=True)  13.1 us
    all_to_all x2, starting transfers between devices, sum_at_owner(): lax.all_to_all(pieces, axis, split_axis=0, concat_axis=0, tiled=True)  11.1 us
    all_to_all x1, waiting for transfers between devices, sent_to_all(): return lax.all_to_all(copies, axis, split_axis=0, concat_axis=0, tiled=True)  9.97 us
  transfers between devices with their start and end apart: 5, of which 5 were waited for; matrix products, arithmetic and copies ran while one was open for 2% of the time, Pallas kernels for 0%

commit v1 on v0

v1 whole, which is shorter than its diff:
```python
import functools

import jax
import jax.numpy as jnp
from jax import lax
from jax.experimental import pallas as pl
from jax.experimental.pallas import tpu as pltpu
from jax.sharding import PartitionSpec as P

PLAIN_KEY_WIDTH = 128
SMALL_HEAD_WIDTH = 64
ROPE = 64
TOK = 112
PAD = 128
CAP = 16
N_SP = 32
N_TP = 16
N_Z = 16
SLOTS = N_SP * CAP
HALF = SLOTS // 2
D = 2048

rope_base = 10000.0
epsilon = 1e-06
very_low = -1e30

MESH = pl.DeviceIdType.MESH
BF = jnp.bfloat16
F32 = jnp.float32

CHUNK = 416
SUBS = ((0, 112), (112, 112), (224, 96), (320, 96))


def dot(a, b):
    return jnp.dot(a, b, preferred_element_type=F32)


def dot_nt(a, b):
    return lax.dot_general(a, b, (((1,), (1,)), ((), ())), preferred_element_type=F32)


def remote(src, dst, send_sem, recv_sem, device):
    return pltpu.make_async_remote_copy(
        src_ref=src, dst_ref=dst, send_sem=send_sem, recv_sem=recv_sem,
        device_id=device, device_id_type=MESH,
    )


def pad_rows(x):
    return jnp.concatenate([x, jnp.zeros((PAD - x.shape[0], x.shape[1]), x.dtype)], axis=0)


def rows16(i):
    return pl.ds(pl.multiple_of(i * CAP, CAP), CAP)


def lanes128(i):
    return pl.ds(pl.multiple_of(i * 128, 128), 128)


def kernel(
    latent, lat_scale, rk2, cs, sn, qw, qw2, qn, lkl, lvl, sv, ids, gain, router_t,
    residual, out_wide, out_narrow, gate_w, up_w, down_w,
    out,
    q, kv, m_s, l_s, accw, accn, ow, wg, wu, wd, resid,
    ps, pr, mixed, ssr, dsel, psel, zs, xg, lgr, hid, ys,
    rb1u, rb1d, rb2u, rb2d, sa, ra1u, ra1d, ra2u, ra2d, res, zr,
    w_sem, ring_s, ring_r, dd_s, dd_r, rs_s, rs_r, ss_s, ss_r, z_s, z_r, loc,
    lg_s, lg_r, xg_s, xg_r, b_s, b_r, a_s, a_r, y_s, y_r,
):
    sp = lax.axis_index("sp")
    tp = lax.axis_index("tp")
    z = sp // 2
    c = sp % 2
    a = (1 - c) * (tp % 4) + c * (tp // 4)
    b = (1 - c) * (tp // 4) + c * (tp % 4)

    def at_ab(aa, bb):
        return (sp, bb * (4 - 3 * c) + aa * (1 + 3 * c))

    def tp_of(aa, bb):
        return bb * (4 - 3 * c) + aa * (1 + 3 * c)

    up_z = (((z + 1) % N_Z) * 2 + c, tp)
    down_z = (((z + N_Z - 1) % N_Z) * 2 + c, tp)
    partner = (z * 2 + 1 - c, tp)

    loads = [
        pltpu.make_async_copy(out_wide, ow.at[pl.ds(0, 128)], w_sem.at[0]),
        pltpu.make_async_copy(out_narrow, ow.at[pl.ds(128, 64)], w_sem.at[1]),
        pltpu.make_async_copy(residual.at[:, lanes128(tp)], resid, w_sem.at[2]),
        pltpu.make_async_copy(gate_w.at[0], wg, w_sem.at[3]),
        pltpu.make_async_copy(up_w.at[0], wu, w_sem.at[4]),
        pltpu.make_async_copy(down_w.at[0], wd, w_sem.at[5]),
    ]
    for load in loads:
        load.start()

    barrier = pltpu.get_barrier_semaphore()

    @pl.loop(1, N_SP)
    def _(k):
        pl.semaphore_signal(barrier, inc=1, device_id=((sp + k) % N_SP, tp), device_id_type=MESH)

    @pl.loop(1, N_TP)
    def _(k):
        pl.semaphore_signal(barrier, inc=1, device_id=(sp, (tp + k) % N_TP), device_id_type=MESH)

    lane = lax.broadcasted_iota(jnp.int32, (TOK, 128), 1)

    def roped(v):
        v = v.astype(F32)
        other = jnp.where(lane < 96, pltpu.roll(v, 96, 1), pltpu.roll(v, 32, 1))
        return v * cs[...] + other * sn[...]

    lat = latent[...].astype(F32)
    normed = lat * lax.rsqrt(jnp.mean(lat * lat, axis=-1, keepdims=True) + epsilon) * lat_scale[...]
    normed = pad_rows(normed.astype(BF))
    kv[sp, pl.ds(0, TOK), :] = dot(normed, lkl[...])[:TOK].astype(BF)
    small = dot(normed, sv[...])
    kv[sp, pl.ds(112, TOK), :] = jnp.where(lane < 64, small[:TOK], roped(rk2[...])).astype(BF)
    kv[sp, pl.ds(224, 128), :] = dot(normed, lvl[...]).T.astype(BF)
    kv[sp, pl.ds(352, 64), :] = small.T[64:].astype(BF)

    q[...] = jnp.zeros_like(q)
    q[pl.ds(0, TOK), pl.ds(0, 128)] = qw[...]
    q[pl.ds(0, TOK), pl.ds(128, 128)] = roped(qw2[...]).astype(BF)
    q[pl.ds(128, TOK), pl.ds(128, 128)] = roped(qn[...]).astype(BF)
    ow[pl.ds(192, 64), :] = jnp.zeros((64, D), BF)

    pl.semaphore_wait(barrier, N_SP - 1 + N_TP - 1)

    def ring_copy(direction, t, sub):
        at, count = SUBS[sub]
        step = t - 1
        origin = (z - step + N_Z) % N_Z if direction == 0 else (z + step) % N_Z
        ref = kv.at[origin * 2 + c, pl.ds(at, count)]
        return remote(ref, ref, ring_s.at[direction, t, sub], ring_r.at[direction, t, sub],
                      up_z if direction == 0 else down_z)

    def across(direction, t):
        origin = (z - t + N_Z) % N_Z if direction == 0 else (z + t) % N_Z
        ref = kv.at[origin * 2 + c]
        return remote(ref, ref, dd_s.at[direction, t], dd_r.at[direction, t], partner)

    for sub in range(4):
        ring_copy(0, 1, sub).start()
        ring_copy(1, 1, sub).start()
    across(0, 0).start()

    lane_q = lax.broadcasted_iota(jnp.int32, (1, 256), 1)
    scale = jnp.where(lane_q < 128, F32(192 ** -0.5), F32(128 ** -0.5))
    m_s[...] = jnp.full_like(m_s, very_low)
    l_s[...] = jnp.zeros_like(l_s)
    accw[...] = jnp.zeros_like(accw)
    accn[...] = jnp.zeros_like(accn)

    def attend(slot, own):
        keys = jnp.concatenate([kv[slot, pl.ds(0, TOK), :], kv[slot, pl.ds(112, TOK), :]], axis=1)
        s = dot_nt(keys, q[...]) * scale
        if own:
            key_at = lax.broadcasted_iota(jnp.int32, (TOK, 256), 0)
            query_at = lax.broadcasted_iota(jnp.int32, (TOK, 256), 1) % 128
            s = jnp.where(key_at <= query_at, s, very_low)
        old = m_s[...]
        new = jnp.maximum(old, jnp.max(s, axis=0, keepdims=True))
        w = jnp.exp(s - new)
        fade = jnp.exp(old - new)
        m_s[...] = new
        l_s[...] = l_s[...] * fade + jnp.sum(w, axis=0, keepdims=True)
        low = pad_rows(w.astype(BF))
        accw[...] = accw[...] * fade[:, :128] + dot(kv[slot, pl.ds(224, 128), :], low[:, :128])
        accn[...] = accn[...] * fade[:, 128:] + dot(kv[slot, pl.ds(352, 64), :], low[:, 128:])

    attend(sp, True)

    id0 = ids[pl.ds(0, 1), :]
    id1 = ids[pl.ds(1, 1), :]
    expert_at = lax.broadcasted_iota(jnp.int32, (N_SP, PAD), 0)
    hot0 = (expert_at == id0).astype(F32)
    hot1 = (expert_at == id1).astype(F32)
    before = (
        lax.broadcasted_iota(jnp.int32, (PAD, PAD), 0) < lax.broadcasted_iota(jnp.int32, (PAD, PAD), 1)
    ).astype(F32).astype(BF)
    earlier = dot((hot0 + hot1).astype(BF), before)
    target0 = id0 * CAP + jnp.sum(earlier * hot0, axis=0, keepdims=True).astype(jnp.int32)
    target1 = id1 * CAP + jnp.sum(earlier * hot1, axis=0, keepdims=True).astype(jnp.int32)
    slot_at = lax.broadcasted_iota(jnp.int32, (SLOTS, PAD), 0)
    dsel[...] = ((slot_at == target0) | (slot_at == target1)).astype(F32).astype(BF)

    def column(row):
        return jnp.broadcast_to(row, (PAD, PAD)).T

    for k, target in ((0, target0), (1, target1)):
        turned = column(target.astype(F32)).astype(jnp.int32)
        for part in range(4):
            lane_at = lax.broadcasted_iota(jnp.int32, (PAD, 128), 1) + part * 128
            psel[k, :, pl.ds(part * 128, 128)] = (lane_at == turned).astype(F32).astype(BF)

    def pending(k, step):
        direction = k % 2
        origin = z - step if direction == 0 else z + step - N_Z
        mine = k < 2
        slot = jnp.maximum(origin, 0) * 2 + (c if mine else 1 - c)
        if mine:
            ok = (origin >= 0) & (step >= 1)
        else:
            ok = (origin >= 0) & ((step >= 1) | (c == 1))
            if direction == 0:
                across(0, step).wait_recv()
            else:
                pl.when(step >= 1)(lambda: across(1, step).wait_recv())

        @pl.when(ok)
        def _():
            attend(slot, False)

    @pl.loop(1, 9)
    def _(t):
        for sub in range(4):
            ring_copy(0, t, sub).wait_recv()

            @pl.when(t < 8)
            def _():
                ring_copy(0, t + 1, sub).start()
                ring_copy(1, t, sub).wait_recv()

            @pl.when(t < 7)
            def _():
                ring_copy(1, t + 1, sub).start()

            if sub == 3:
                across(0, t).start()

                @pl.when(t < 8)
                def _():
                    across(1, t).start()

            pending(sub, t - 1)

    pending(0, 8)
    pending(2, 8)

    loads[0].wait()
    loads[1].wait()
    loads[2].wait()
    total = l_s[...]
    heads_w = (accw[...] / total[:, :128]).T
    heads_n = pad_rows(accn[...] / total[:, 128:]).T
    heads = jnp.concatenate([heads_w, heads_n], axis=1).astype(BF)
    for j in range(8):
        part = dot(heads, ow[:, pl.ds(j * 256, 256)]).astype(BF)
        ps[2 * j] = part[:TOK, :128]
        ps[2 * j + 1] = part[:TOK, 128:]

    def rs_copy(k):
        to = (tp + k) % N_TP
        return remote(ps.at[to], pr.at[k], rs_s.at[k], rs_r.at[k], (sp, to))

    @pl.loop(1, N_TP)
    def _(k):
        rs_copy(k).start()

    mixed[...] = resid[...].astype(F32) + ps[tp].astype(F32)

    @pl.loop(1, N_TP)
    def _(k):
        rs_copy(k).wait_recv()
        mixed[...] += pr[k].astype(F32)

    mix = pad_rows(mixed[...])
    ssr[0] = jnp.broadcast_to(jnp.sum((mix * mix).T, axis=0, keepdims=True), (8, PAD))

    def ss_copy(k):
        return remote(ssr.at[0], ssr.at[k], ss_s.at[k], ss_r.at[k], (sp, (tp + k) % N_TP))

    @pl.loop(1, N_TP)
    def _(k):
        ss_copy(k).start()

    @pl.loop(1, N_TP)
    def _(k):
        ss_copy(k).wait_recv()

    squares = jnp.sum(ssr[...], axis=0)[:1]
    inverse = column(lax.rsqrt(squares * (1.0 / D) + epsilon))
    normal = (mix * inverse * gain[pl.ds(tp, 1), :]).astype(BF)

    zs[...] = dot(dsel[...], normal).astype(BF)

    def far_first(i):
        return N_Z + (1 - 2 * (i % 2)) * ((i + 1) // 2)

    def z_copy(k):
        to = (sp + k) % N_SP
        return remote(zs.at[rows16(to)], xg.at[rows16(sp), lanes128(tp)], z_s.at[k], z_r.at[k], (to, tp))

    @pl.loop(0, N_SP - 1)
    def _(i):
        z_copy(far_first(i)).start()

    own_rows = pltpu.make_async_copy(zs.at[rows16(sp)], xg.at[rows16(sp), lanes128(tp)], loc.at[0])
    own_rows.start()

    lgr[0] = dot_nt(router_t[...], normal)

    def lg_copy(k):
        return remote(lgr.at[0], lgr.at[k], lg_s.at[k], lg_r.at[k], (sp, (tp + k) % N_TP))

    @pl.loop(1, N_TP)
    def _(k):
        lg_copy(k).start()

    @pl.loop(1, N_SP)
    def _(k):
        z_copy(k).wait_recv()

    own_rows.wait()

    right_a, left_a = at_ab((a + 1) % 4, b), at_ab((a + 3) % 4, b)
    right_b, left_b = at_ab(a, (b + 1) % 4), at_ab(a, (b + 3) % 4)
    column_a = (a, (a + 3) % 4, (a + 1) % 4, (a + 2) % 4)

    def gather_copy(n, aa, bb, half, device):
        rows = pl.ds(0, SLOTS) if half is None else pl.ds(half * HALF, HALF)
        ref = xg.at[rows, lanes128(tp_of(aa, bb))]
        return remote(ref, ref, xg_s.at[n], xg_r.at[n], device)

    started = []

    def send(n, *rest):
        copy = gather_copy(n, *rest)
        copy.start()
        started.append(copy)

    send(0, a, b, None, right_a)
    send(1, a, b, None, left_a)
    send(4, a, b, None, right_b)
    send(5, a, b, None, left_b)
    from_left, from_right = (a + 3) % 4, (a + 1) % 4
    opposite = (a + 2) % 4
    gather_copy(0, from_left, b, None, right_a).wait_recv()
    send(2, from_left, b, 0, right_a)
    send(8, from_left, b, None, right_b)
    send(9, from_left, b, None, left_b)
    gather_copy(1, from_right, b, None, left_a).wait_recv()
    send(3, from_right, b, 1, left_a)
    send(12, from_right, b, None, right_b)
    send(13, from_right, b, None, left_b)
    down_b, up_b, far_b = (b + 3) % 4, (b + 1) % 4, (b + 2) % 4

    def relay(i):
        gather_copy(4 + 4 * i, column_a[i], down_b, None, right_b).wait_recv()
        send(6 + 4 * i, column_a[i], down_b, 0, right_b)
        gather_copy(5 + 4 * i, column_a[i], up_b, None, left_b).wait_recv()
        send(7 + 4 * i, column_a[i], up_b, 1, left_b)

    relay(0)
    gather_copy(2, opposite, b, 0, right_a).wait_recv()
    gather_copy(3, opposite, b, 1, left_a).wait_recv()
    send(16, opposite, b, None, right_b)
    send(17, opposite, b, None, left_b)
    for i in (1, 2, 3):
        relay(i)
    for i in range(4):
        gather_copy(6 + 4 * i, column_a[i], far_b, 0, right_b).wait_recv()
        gather_copy(7 + 4 * i, column_a[i], far_b, 1, left_b).wait_recv()

    for load in loads[3:]:
        load.wait()

    @pl.loop(0, 2)
    def _(i):
        at = pl.ds(pl.multiple_of(i * HALF, HALF), HALF)
        rows = xg[at, :]
        gate = dot(rows, wg[...])
        hid[at, :] = (gate / (1.0 + jnp.exp(-gate)) * dot(rows, wu[...])).astype(BF)

    top, bottom = pl.ds(0, HALF), pl.ds(HALF, HALF)

    def down(db):
        @pl.loop(0, 4)
        def _(da):
            to = tp_of((a + da) % 4, (b + db) % 4)
            ys[db, da] = dot(hid[...], wd[:, lanes128(to)]).astype(BF)

    sums = []

    def give(n, src, dst, sems, device):
        copy = remote(src, dst, sems[0].at[n], sems[1].at[n], device)
        copy.start()
        sums.append(copy)
        return copy

    bs, as_ = (b_s, b_r), (a_s, a_r)
    down(2)
    far = {}
    for da in range(4):
        far[da] = (
            give(da, ys.at[2, da, top], rb2u.at[da], bs, right_b),
            give(4 + da, ys.at[2, da, bottom], rb2d.at[da], bs, left_b),
        )
    down(1)
    near = {}
    for da in range(4):
        near[da] = [give(8 + da, ys.at[1, da, bottom], rb1u.at[da, bottom], bs, right_b)]
    down(3)
    for da in range(4):
        near[da].append(give(12 + da, ys.at[3, da, top], rb1d.at[da, top], bs, left_b))
    for da in (2, 1, 3, 0):
        far[da][0].wait_recv()
        ys[1, da, top] = (ys[1, da, top].astype(F32) + rb2u[da].astype(F32)).astype(BF)
        near[da].append(give(16 + da, ys.at[1, da, top], rb1u.at[da, top], bs, right_b))
        far[da][1].wait_recv()
        ys[3, da, bottom] = (ys[3, da, bottom].astype(F32) + rb2d[da].astype(F32)).astype(BF)
        near[da].append(give(20 + da, ys.at[3, da, bottom], rb1d.at[da, bottom], bs, left_b))
    down(0)

    def line_sum(da):
        for copy in near[da]:
            copy.wait_recv()
        return ys[0, da].astype(F32) + rb1u[da].astype(F32) + rb1d[da].astype(F32)

    sa[2] = line_sum(2).astype(BF)
    far_a = (
        give(0, sa.at[2, top], ra2u, as_, right_a),
        give(1, sa.at[2, bottom], ra2d, as_, left_a),
    )
    sa[1] = line_sum(1).astype(BF)
    near_a = [give(2, sa.at[1, bottom], ra1u.at[bottom], as_, right_a)]
    sa[3] = line_sum(3).astype(BF)
    near_a.append(give(3, sa.at[3, top], ra1d.at[top], as_, left_a))
    far_a[0].wait_recv()
    sa[1, top] = (sa[1, top].astype(F32) + ra2u[...].astype(F32)).astype(BF)
    near_a.append(give(4, sa.at[1, top], ra1u.at[top], as_, right_a))
    far_a[1].wait_recv()
    sa[3, bottom] = (sa[3, bottom].astype(F32) + ra2d[...].astype(F32)).astype(BF)
    near_a.append(give(5, sa.at[3, bottom], ra1d.at[bottom], as_, left_a))
    own_sum = line_sum(0)
    for copy in near_a:
        copy.wait_recv()
    res[...] = (own_sum + ra1u[...].astype(F32) + ra1d[...].astype(F32)).astype(BF)

    def y_copy(k):
        to = (sp + k) % N_SP
        return remote(res.at[rows16(to)], zr.at[rows16(sp)], y_s.at[k], y_r.at[k], (to, tp))

    @pl.loop(0, N_SP - 1)
    def _(i):
        y_copy(far_first(i)).start()

    own_back = pltpu.make_async_copy(res.at[rows16(sp)], zr.at[rows16(sp)], loc.at[1])
    own_back.start()

    @pl.loop(1, N_TP)
    def _(k):
        lg_copy(k).wait_recv()

    logit = jnp.sum(lgr[...], axis=0)
    row8 = lax.broadcasted_iota(jnp.int32, (8, PAD), 0)
    group = jnp.where(row8 < 4, logit[:8], very_low)
    group = jnp.exp(group - jnp.max(group, axis=0, keepdims=True))
    picked = jnp.sum(jnp.where(row8 == (id0 >> 3), group, 0.0), axis=0, keepdims=True)
    pick = picked / jnp.sum(group, axis=0, keepdims=True)
    logit0 = jnp.sum(jnp.where(expert_at == id0, logit[8:], 0.0), axis=0, keepdims=True)
    logit1 = jnp.sum(jnp.where(expert_at == id1, logit[8:], 0.0), axis=0, keepdims=True)
    peak = jnp.maximum(logit0, logit1)
    e0, e1 = jnp.exp(logit0 - peak), jnp.exp(logit1 - peak)
    gate0 = column(pick * e0 / (e0 + e1))
    gate1 = column(pick * e1 / (e0 + e1))

    @pl.loop(1, N_SP)
    def _(k):
        y_copy(k).wait_recv()

    own_back.wait()
    back = zr[...]
    done = pad_rows(mixed[...]) + (gate0 * dot(psel[0], back) + gate1 * dot(psel[1], back))
    out[...] = done[:TOK].astype(BF)

    @pl.loop(1, 9)
    def _(t):
        for sub in range(4):
            ring_copy(0, t, sub).wait_send()
            pl.when(t < 8)(lambda: ring_copy(1, t, sub).wait_send())
        across(0, t).wait_send()
        pl.when(t < 8)(lambda: across(1, t).wait_send())

    across(0, 0).wait_send()

    @pl.loop(1, N_TP)
    def _(k):
        rs_copy(k).wait_send()
        ss_copy(k).wait_send()
        lg_copy(k).wait_send()

    @pl.loop(1, N_SP)
    def _(k):
        z_copy(k).wait_send()
        y_copy(k).wait_send()

    for copy in started + sums:
        copy.wait_send()


def layer(*args):
    vmem = pl.BlockSpec(memory_space=pltpu.VMEM)
    anywhere = pl.BlockSpec(memory_space=pl.ANY)
    dma = pltpu.SemaphoreType.DMA

    def v(*shape, dtype=BF):
        return pltpu.VMEM(shape, dtype)

    return pl.pallas_call(
        kernel,
        out_shape=jax.ShapeDtypeStruct((TOK, 128), BF),
        in_specs=[vmem] * 14 + [anywhere] * 6,
        out_specs=vmem,
        scratch_shapes=[
            v(256, 256), v(N_SP, CHUNK, 128), v(1, 256, dtype=F32), v(1, 256, dtype=F32),
            v(128, 128, dtype=F32), v(64, 128, dtype=F32),
            v(256, D), v(D, 256), v(D, 256), v(256, D), v(TOK, 128),
            v(N_TP, TOK, 128), v(N_TP, TOK, 128), v(TOK, 128, dtype=F32), v(N_TP, 8, 128, dtype=F32),
            v(SLOTS, 128), v(2, PAD, SLOTS), v(SLOTS, 128), v(SLOTS, D), v(N_TP, 40, 128, dtype=F32),
            v(SLOTS, 256), v(4, 4, SLOTS, 128),
            v(4, SLOTS, 128), v(4, SLOTS, 128), v(4, HALF, 128), v(4, HALF, 128),
            v(4, SLOTS, 128), v(SLOTS, 128), v(SLOTS, 128), v(HALF, 128), v(HALF, 128),
            v(SLOTS, 128), v(SLOTS, 128),
            dma((6,)), dma((2, 9, 4)), dma((2, 9, 4)), dma((2, 9)), dma((2, 9)),
            dma((N_TP,)), dma((N_TP,)), dma((N_TP,)), dma((N_TP,)), dma((N_SP,)), dma((N_SP,)), dma((2,)),
            dma((N_TP,)), dma((N_TP,)), dma((20,)), dma((20,)), dma((24,)), dma((24,)),
            dma((6,)), dma((6,)), dma((N_SP,)), dma((N_SP,)),
        ],
        compiler_params=pltpu.CompilerParams(
            collective_id=0, has_side_effects=True, vmem_limit_bytes=48 * 1024 * 1024
        ),
        name="layer",
    )(*args)


def shards(
    residual, latent, rot_key, latent_norm_scale, query_wide, query_narrow,
    large_key_lift, large_value_lift, small_key_lift, small_value_lift,
    out_wide, out_narrow, mix_gain, router_group, router_expert, expert_ids,
    expert_gate_w, expert_up_w, expert_down_w,
):
    tp = lax.axis_index("tp")
    positions = lax.axis_index("sp") * TOK + jnp.arange(TOK, dtype=jnp.int32)
    frequency = rope_base ** (-jnp.arange(0, ROPE, 2, dtype=F32) / ROPE)
    angles = positions.astype(F32)[:, None] * frequency[None, :]
    cosine, sine = jnp.cos(angles), jnp.sin(angles)
    cs = jnp.concatenate([jnp.ones((TOK, 64), F32), cosine, cosine], axis=1)
    sn = jnp.concatenate([jnp.zeros((TOK, 64), F32), -sine, sine], axis=1)
    blank = jnp.zeros((TOK, 64), BF)
    rk2 = jnp.concatenate([blank, rot_key], axis=1)
    qw = query_wide[:, :128]
    qw2 = jnp.concatenate([blank, query_wide[:, 128:]], axis=1)
    sv = jnp.concatenate([small_key_lift, small_value_lift], axis=1)
    ids = jnp.pad(expert_ids.T, ((0, 6), (0, PAD - TOK)), constant_values=-1)
    router = jnp.concatenate([router_group, jnp.zeros((D, 4), BF), router_expert], axis=1)
    router_t = lax.dynamic_slice_in_dim(router, tp * 128, 128, 0).T
    return layer(
        latent, latent_norm_scale.reshape(1, -1), rk2, cs, sn, qw, qw2, query_narrow,
        large_key_lift, large_value_lift, sv, ids, mix_gain.reshape(N_TP, 128), router_t,
        residual, out_wide, out_narrow, expert_gate_w, expert_up_w, expert_down_w,
    )


def solution(mesh):
    placed = (
        P("sp", None), P("sp", None), P("sp", None), P(), P("sp", "tp"), P("sp", "tp"),
        P(None, "tp"), P(None, "tp"), P(None, "tp"), P(None, "tp"), P("tp", None), P("tp", None),
        P(), P(), P(), P("sp", None),
        P("sp", None, "tp"), P("sp", None, "tp"), P("sp", "tp", None),
    )
    return jax.shard_map(
        shards, mesh=mesh, in_specs=placed, out_specs=P("sp", "tp"), check_vma=False
    )
```

time: 287 us -> 136 us (0.47)
  waiting for transfers between devices: 136 us -> 0 us
  Pallas kernels: 0 us -> 121 us
  blocking collectives: 55.8 us -> 0 us
  starting transfers between devices: 27.8 us -> 0 us
  matrix products: 23.1 us -> 0 us
  between operations: 13.8 us -> 0.16 us
  other arithmetic: 10.3 us -> 1.31 us
  local copies, waits for them, and re-layouts: 18.7 us -> 12.8 us
    pallas_call x0 -> x1, Pallas kernels: none -> 121 us  [layer(): pl.pallas_call(kernel, out_shape=jax.ShapeDtypeStruct((TOK, 128), BF), in...]
    all_gather x1 -> x0, waiting for transfers between devices: 76.9 us -> none  [sent_together(): out, at, done = (lax.all_gather(both, axis, axis=dim, tiled=True), 0, [])]
    all_to_all x4 -> x0, waiting for transfers between devices: 59.2 us -> none  [the longest x2 33.6 us: sum_at_owner(): lax.all_to_all(pieces, axis, split_axis=0, concat_axis=0, tiled=True)]
    all_to_all x2 -> x0, blocking collectives: 55.8 us -> none  [the longest x1 30 us: sent_to_all(): return lax.all_to_all(copies, axis, split_axis=0, concat_axis=0, tiled=True)]
    all_to_all x4 -> x0, starting transfers between devices: 27.8 us -> none  [the longest x1 13.1 us: shards(): lax.all_to_all(shaped_out, 'sp', split_axis=2, concat_axis=0, tiled=True)]
    dot_general x14 -> x0, matrix products: 23.1 us -> none  [the longest x1 5.65 us: shards(): jnp.einsum('erf,efd->erd', hidden, expert_down_w, preferred_element_type=...]
    unnamed x33 -> x30, local copies, waits for them, and re-layouts: 2.98 us -> 10.4 us
    reduce_sum x11 -> x0, other arithmetic: 4.44 us -> none  [the longest x2 2 us: sum_at_owner(): return arrived.astype(jnp.float32).sum(axis=0)]
  transfers between devices with their start and end apart: 5 -> 0, of which waited for: 5 -> 0; matrix products, arithmetic and copies ran while one was open for 2% -> 0% of each run, Pallas kernels for 0% -> 0%
where the time goes in v1:
time: 136 us; the launch traced here: 135 us
  Pallas kernels  121 us (89%)
  local copies, waits for them, and re-layouts  12.8 us (9%)
    pallas_call x1, Pallas kernels, layer(): pl.pallas_call(kernel, out_shape=jax.ShapeDtypeStruct((TOK, 128), BF), in...  121 us
    unnamed x30, local copies, waits for them, and re-layouts  10.4 us

profile of v1, /device:TPU:1, one launch (start us, length us, event | category | flops | bytes accessed | tf_op | source)
XLA Modules:
  0.0 135.1 jit_solution(3505905083013973323)
XLA Ops:
  0.0 0.3 fusion
  0.4 0.1 pad_maximum_fusion.1
  0.5 0.1 pad.8.clone
  0.6 0.8 fusion.2.router_t
  1.4 1.0 copy.29
  2.3 1.0 copy.30
  3.4 0.1 pad_maximum_fusion.sv
  3.5 0.7 slice.7
  4.2 0.1 copy.32
  4.3 0.1 concatenate.21.qw2
  4.4 0.8 slice.6
  5.2 0.1 copy.31.qw
  5.3 0.8 copy.25
  6.1 0.1 concatenate.18.rk2
  6.2 0.7 pad.6.ids
  7.0 0.6 copy-done.11
  7.6 1.2 copy-done.1
  8.9 1.2 copy-done.2
  10.1 1.0 copy-done.4
  11.1 0.9 copy-done.5
  12.0 0.9 copy-done.7
  13.0 0.7 copy-done.9
  13.7 120.8 %layer.1 = bf16[112,128]{1,0:T(8,128)(2,1)S(1)} custom-call(bf16[112,512]{1,0:T(8,128)(2,1)S(1)} %copy-done.8, f32[1,512]{1,0:T(1,128)S(1)} %bitcast.6, bf16[112,128]{1,0:T(8,128)(2,1)S(1)} %concatenate.18.rk2, f32[112,128]{1,0:T(8,128)S(1)} %get-tuple-element.8.cs, f32[112,128]{1,0:T(8,128)S(1)} %get-tuple-element.9.sn, bf16[112,128]{1,0:T(8,128)(2,1)S(1)} %copy.31.qw, ...), custom_call_target="tpu_custom_call" | custom-call | tf_op jit(solution)/shard_map/layer/pallas_call | solution.py:515
  134.5 0.6 copy.34
  (24 shorter events, 0.1 us)
Async XLA Ops:
  0.0 6.9 %copy-start = (bf16[1,2048,256]{2,1,0:T(8,128)(2,1)S(1)}, bf16[1,2048,256]{2,1,0:T(8,128)(2,1)}, u32[]{:S(2)}) copy-start(bf16[1,2048,256]{2,1,0:T(8,128)(2,1)} %gate_w.1) | copy-start | bytes 3145732
  2.3 4.6 %copy-start.3 = (bf16[128,2048]{1,0:T(8,128)(2,1)S(1)}, bf16[128,2048]{1,0:T(8,128)(2,1)}, u32[]{:S(2)}) copy-start(bf16[128,2048]{1,0:T(8,128)(2,1)} %out_wide.1) | copy-start | bytes 1572868
  4.3 2.6 %copy-start.8 = (bf16[112,512]{1,0:T(8,128)(2,1)S(1)}, bf16[112,512]{1,0:T(8,128)(2,1)}, u32[]{:S(2)}) copy-start(bf16[112,512]{1,0:T(8,128)(2,1)} %latent.1) | copy-start | bytes 344068
  4.4 2.6 %copy-start.6 = (bf16[512,128]{1,0:T(8,128)(2,1)S(1)}, bf16[512,128]{1,0:T(8,128)(2,1)}, u32[]{:S(2)}) copy-start(bf16[512,128]{1,0:T(8,128)(2,1)} %lkl.1) | copy-start | bytes 393220
  6.2 0.7 copy-start.10
  6.9 0.7 copy-start.11
  7.6 1.2 copy-start.1
  8.8 1.2 copy-start.2
  10.1 1.0 copy-start.4
  11.1 0.9 copy-start.5
  12.0 0.9 copy-start.7
  12.9 0.7 copy-start.9
